TPU v7x, 512 devices: a whole 4x4x16 slice. The times are simulated.
512 devices in a mesh: sp: 128 (over z, x, core), tp: 4 (over y).
Axes of the slice: x: 4, y: 4, z: 16, core: 2. Of those that a mesh axis runs over, the one named last changes fastest.
Arguments:
- inputs: bfloat16 [4, 16384, 1024], P(None, 'sp'), may hold values from -6 to 6
- norm_gain: float32 [1024], replicated, may hold values from 0.1 to 1.9
- query_weight: bfloat16 [1024, 3, 8, 64], P('sp', None, 'tp'), may hold values from -0.1875 to 0.1875
- key_weight: bfloat16 [1024, 3, 8, 64], P('sp', None, 'tp'), may hold values from -0.1875 to 0.1875
- value_weight: bfloat16 [1024, 3, 8, 64], P('sp', None, 'tp'), may hold values from -0.1875 to 0.1875
- query_gain: float32 [3, 64], replicated, may hold values from 0.1 to 1.9
- key_gain: float32 [3, 64], replicated, may hold values from 0.1 to 1.9
- out_weight: bfloat16 [8, 64, 1024], P('tp', None, 'sp'), may hold values from -0.75 to 0.75
Outputs:
- mixed: bfloat16 [4, 16384, 1024], P(None, 'sp', 'tp')
All inputs are finite; a program needn't handle non-finite values.
Results may differ from a plain program's by a relative error of at most 0.02.
Values may be sent and summed in bfloat16 or wider, within the bound.
A program may use at most 64 MiB of HBM per device.

v0:
```python
import math
import jax
import jax.numpy as jnp
from jax import lax
from jax.sharding import Mesh
from jax.sharding import PartitionSpec as P

SPAN_CLOSE = 32
SPREAD_CENTRAL = 4
SPAN_CENTRAL = 32
SPREAD_DISTANT = 16
SPAN_DISTANT = 16
SP = ("sp_0", "sp_1", "sp_2")
eps = 1e-06
neg_fill = -1e30


def joined_along(tiles, dim):
    tiles = jnp.moveaxis(tiles, 0, dim)
    shape = tiles.shape
    return tiles.reshape(*shape[:dim], shape[dim] * shape[dim + 1], *shape[dim + 2 :])


def stacked_from(value, axes, sequence):
    tiles = value[None]
    for k in sequence:
        tiles = lax.all_gather(tiles, axes[k], axis=0, tiled=True)
    block = [lax.axis_size(axes[k]) for k in reversed(sequence)]
    tiles = tiles.reshape(*block, *value.shape)
    turned = sorted(range(len(sequence)), key=lambda place: sequence[len(sequence) - 1 - place])
    return tiles.transpose(*turned, *range(len(sequence), tiles.ndim)).reshape(-1, *value.shape)


def gather_axes(value, axes, sequence, dim):
    return joined_along(stacked_from(value, axes, sequence), dim)


def over_axes(value, axes, sequence, dim, take_in, carry):
    everything = jax.tree.map(lambda part: gather_axes(part, axes, sequence, dim), value)
    return take_in(carry, everything, jnp.int32(0))


def padded(cells, sides, width, closed):
    for axis, dim in sides:
        count = lax.axis_size(axis)
        ends = count if closed else count - 1
        head = lax.slice_in_dim(cells, 0, width, axis=dim)
        tail = lax.slice_in_dim(cells, cells.shape[dim] - width, cells.shape[dim], axis=dim)
        cells = jnp.concatenate(
            [
                lax.ppermute(tail, axis, [(i, (i + 1) % count) for i in range(ends)]),
                cells,
                lax.ppermute(head, axis, [((i + 1) % count, i) for i in range(ends)]),
            ],
            axis=dim,
        )
    return cells


def shifted(block, axis, distance):
    devices = range(lax.axis_size(axis))
    route = [(i - distance, i) for i in devices if i - distance in devices]
    return lax.ppermute(block, axis, route)


def on_whole(value, axes, sequence, dim, apply):
    return apply(gather_axes(value, axes, sequence, dim), jnp.int32(0))


def row_norm(values, gain):
    scaled = values * lax.rsqrt(jnp.mean(values * values, axis=-1, keepdims=True) + eps)
    return scaled * gain


def band_attend(queries, keys, values, margin, dilation, half, slopes, anchor, seq_len):
    batch, count, heads, width = queries.shape
    query_rows = count // dilation
    key_rows = query_rows + 2 * half
    first = margin - half * dilation
    keys = keys[:, first : first + key_rows * dilation]
    values = values[:, first : first + key_rows * dilation]
    query_sub = queries.reshape(batch, query_rows, dilation, heads, width)
    key_sub = keys.reshape(batch, key_rows, dilation, heads, width)
    value_sub = values.reshape(batch, key_rows, dilation, heads, width)
    scores = jnp.einsum(
        "barhe,bcrhe->brhac", query_sub, key_sub, precision=lax.Precision.DEFAULT
    ) / math.sqrt(width)
    offset = jnp.arange(key_rows)[None, :] - half - jnp.arange(query_rows)[:, None]
    key_place = (
        anchor + first + dilation * jnp.arange(key_rows)[None, :] + jnp.arange(dilation)[:, None]
    )
    inside = (key_place >= 0) & (key_place < seq_len)
    allowed = (jnp.abs(offset) <= half)[None, :, :] & inside[:, None, :]
    slant = -slopes[:, None, None] * (jnp.abs(offset).astype(jnp.float32) / float(half))[None]
    scores = jnp.where(allowed[None, :, None], scores + slant[None, None], neg_fill)
    log_total = jax.nn.logsumexp(scores, axis=-1)
    weights = jnp.exp(scores - log_total[..., None])
    result = jnp.einsum("brhac,bcrhe->barhe", weights, value_sub, precision=lax.Precision.DEFAULT)
    log_total = jnp.transpose(log_total, (0, 3, 1, 2)).reshape(batch, count, heads)
    return (result.reshape(batch, count, heads, width), log_total)


def assemble(own, fetched, reach):
    before = [fetched[distance] for distance in range(reach, 0, -1)]
    after = [fetched[-distance] for distance in range(1, reach + 1)]
    return jnp.concatenate(before + [own] + after, axis=1)


def body(
    inputs, norm_gain, query_weight, key_weight, value_weight, query_gain, key_gain, out_weight
):
    batch, local_sequence_count, model_width = inputs.shape
    groups = query_weight.shape[1]
    heads_here = query_weight.shape[2]
    head_width = query_weight.shape[3]
    seq_len = local_sequence_count * lax.axis_size(SP)
    place = lax.axis_index(SP) * local_sequence_count
    flat = inputs.reshape(batch * local_sequence_count, model_width).astype(jnp.float32)
    normed = row_norm(flat, norm_gain).astype(jnp.bfloat16)
    empty = jnp.zeros((batch * local_sequence_count, groups * heads_here * head_width), jnp.float32)

    def add_rows(totals, pieces, start):
        rows = pieces[0].shape[0]
        columns = lax.dynamic_slice_in_dim(normed, start, rows, 1)
        return tuple(
            (
                total
                + jnp.dot(columns, piece.reshape(rows, -1), preferred_element_type=jnp.float32)
                for total, piece in zip(totals, pieces)
            )
        )

    projected = over_axes(
        (query_weight, key_weight, value_weight),
        (("sp_0", "sp_1"), "sp_2"),
        (0, 1),
        0,
        add_rows,
        (empty, empty, empty),
    )
    layout = (batch, local_sequence_count, groups, heads_here, head_width)
    queries = projected[0].astype(jnp.bfloat16).reshape(layout)
    keys = projected[1].astype(jnp.bfloat16).reshape(layout)
    values = projected[2].astype(jnp.bfloat16).reshape(layout)
    pairs = jnp.concatenate([keys, values], axis=-1)
    total_heads = heads_here * lax.axis_size("tp")
    head_index = lax.axis_index("tp") * heads_here + jnp.arange(heads_here)
    slopes = jnp.exp2(-8.0 * (head_index + 1).astype(jnp.float32) / total_heads)
    central_extent = (
        SPREAD_CENTRAL * SPAN_CENTRAL + local_sequence_count - 1
    ) // local_sequence_count
    distant_extent = (
        SPREAD_DISTANT * SPAN_DISTANT + local_sequence_count - 1
    ) // local_sequence_count
    near_window = padded(pairs[:, :, 0], ((SP, 1),), SPAN_CLOSE, False)
    mid_fetched = {}
    far_fetched = {}
    for distance in range(1, central_extent + 1):
        for direction in (1, -1):
            both = shifted(pairs[:, :, 1:], SP, direction * distance)
            mid_fetched[direction * distance] = both[:, :, 0]
            far_fetched[direction * distance] = both[:, :, 1]
    for distance in range(central_extent + 1, distant_extent + 1):
        for direction in (1, -1):
            far_fetched[direction * distance] = shifted(pairs[:, :, 2], SP, direction * distance)
    central_span_width = assemble(pairs[:, :, 1], mid_fetched, central_extent)
    distant_span_width = assemble(pairs[:, :, 2], far_fetched, distant_extent)
    settings = (
        (near_window, SPAN_CLOSE, 1, SPAN_CLOSE),
        (central_span_width, central_extent * local_sequence_count, SPREAD_CENTRAL, SPAN_CENTRAL),
        (distant_span_width, distant_extent * local_sequence_count, SPREAD_DISTANT, SPAN_DISTANT),
    )
    results = []
    totals = []
    for group in range(3):
        window, margin, dilation, half = settings[group]
        query_group = row_norm(queries[:, :, group].astype(jnp.float32), query_gain[group])
        key_group = row_norm(window[..., :head_width].astype(jnp.float32), key_gain[group])
        value_group = window[..., head_width:].astype(jnp.float32)
        result, log_total = band_attend(
            query_group,
            key_group,
            value_group,
            margin,
            dilation,
            half,
            slopes,
            place - margin,
            seq_len,
        )
        results.append(result)
        totals.append(log_total)
    weights = jax.nn.softmax(jnp.stack(totals, 0), axis=0)
    combined = jnp.sum(weights[..., None] * jnp.stack(results, 0), axis=0)
    merged = combined.astype(jnp.bfloat16).reshape(
        batch * local_sequence_count, heads_here * head_width
    )

    def project(piece, start):
        return jnp.dot(merged, piece, preferred_element_type=jnp.float32)

    terms = on_whole(out_weight.reshape(heads_here * head_width, -1), SP, (0, 1, 2), 1, project)
    summed = lax.psum_scatter(
        terms.astype(jnp.bfloat16), "tp", scatter_dimension=1, tiled=True
    ).astype(jnp.float32)
    return summed.astype(jnp.bfloat16).reshape(batch, local_sequence_count, -1)


def solution(mesh):
    finer = Mesh(mesh.devices.reshape(16, 4, 2, mesh.shape["tp"]), ("sp_0", "sp_1", "sp_2", "tp"))
    placed = (
        P(None, SP, None),
        P(),
        P(SP, None, "tp", None),
        P(SP, None, "tp", None),
        P(SP, None, "tp", None),
        P(),
        P(),
        P("tp", None, SP),
    )
    return jax.shard_map(
        body, mesh=finer, in_specs=placed, out_specs=P(None, SP, "tp"), check_vma=False
    )
```

profile of v0, /device:TPU:2, one launch (start us, length us, event | category | flops | bytes accessed | tf_op | source)
XLA Modules:
  0.0 474.6 jit_solution(8545988568318055102)
XLA Ops:
  6.5 1.5 fusion.2
  8.0 107.0 %all-gather.1 = bf16[512,3,2,64]{3,2,1,0:T(2,128)(2,1)S(1)} all-gather(bf16[8,3,2,64]{3,2,1,0:T(2,128)(2,1)} %param.11), channel_id=3, replica_groups=mesh['sp_0'=16,'sp_1'=4,'sp_2'=2,'tp'=4] {'sp_0','sp_1'}, dimensions={0}, use_global_device_ids=true | all-gather | bytes 399360 | tf_op jit(solution)/shard_map/all_gather | solution.py:27
  115.2 2.9 all_gather.30
  118.1 1.2 copy.329
  119.4 1.0 reshape_reshape_reshape.10
  120.4 98.5 %all-gather.2 = bf16[512,3,2,64]{3,2,1,0:T(2,128)(2,1)S(1)} all-gather(bf16[8,3,2,64]{3,2,1,0:T(2,128)(2,1)S(1)} %copy-done.10), channel_id=4, replica_groups=mesh['sp_0'=16,'sp_1'=4,'sp_2'=2,'tp'=4] {'sp_0','sp_1'}, dimensions={0}, use_global_device_ids=true | all-gather | bytes 399360 | tf_op jit(solution)/shard_map/all_gather | solution.py:27
  219.0 2.9 all_gather.32
  221.9 1.2 copy.328
  223.2 1.7 reshape_reshape_reshape.11
  225.3 0.8 copy-done.5
  227.9 1.0 copy.223
  229.3 1.0 copy.224
  230.4 0.8 fusion.57
  231.1 3.9 collective-permute-start.5
  235.1 2.0 collective-permute-start.4
  237.1 0.8 fusion.92
  237.9 2.0 collective-permute-start
  240.0 3.7 collective-permute-start.1
  243.6 0.8 fusion.43
  244.5 3.1 collective-permute-start.3
  252.2 26.8 %all_gather.33 = bf16[16,128,8]{1,2,0:T(8,128)(2,1)S(1)} all-gather(bf16[1,128,8]{1,2,0:T(8,128)(2,1)S(1)} %broadcast_in_dim_reshape.3), channel_id=1, replica_groups=mesh['sp_0'=16,'sp_1'=4,'sp_2'=2,'tp'=4] {'sp_0'}, dimensions={0}, use_global_device_ids=true | all-gather | bytes 34816 | tf_op jit(solution)/shard_map/all_gather | solution.py:27
  279.1 0.8 broadcast_multiply_fusion
  279.8 14.0 %all_gather.34 = bf16[64,128,8]{1,2,0:T(8,128)(2,1)S(1)} all-gather(bf16[16,128,8]{1,2,0:T(8,128)(2,1)S(1)} %all_gather.33), channel_id=1, replica_groups=mesh['sp_0'=16,'sp_1'=4,'sp_2'=2,'tp'=4] {'sp_1'}, dimensions={0}, use_global_device_ids=true | all-gather | bytes 163840 | tf_op jit(solution)/shard_map/all_gather | solution.py:27
  293.8 98.9 %all-gather = bf16[512,3,2,64]{3,2,1,0:T(2,128)(2,1)S(1)} all-gather(bf16[8,3,2,64]{3,2,1,0:T(2,128)(2,1)S(1)} %copy-done.11), channel_id=2, replica_groups=mesh['sp_0'=16,'sp_1'=4,'sp_2'=2,'tp'=4] {'sp_0','sp_1'}, dimensions={0}, use_global_device_ids=true | all-gather | bytes 399360 | tf_op jit(solution)/shard_map/all_gather | solution.py:27
  392.9 3.1 all_gather.28
  396.0 1.2 copy.330
  397.2 1.7 reshape_reshape_reshape.9
  399.0 1.8 convolution_convert_fusion.3
  403.5 0.9 multiply_multiply_fusion
  404.4 1.0 multiply_multiply_fusion.1
  405.5 2.1 all_gather.35
  407.6 0.8 copy.260
  408.4 2.0 collective-permute-start.2
  410.4 1.3 pad_maximum_fusion.1
  412.5 1.0 convolution_bitcast_fusion.1
  413.5 1.0 constant_dynamic-update-slice_fusion.2
  414.5 1.0 slice_bitcast_fusion.2
  415.5 4.4 collective-permute-done.2
  420.7 1.6 fusion.94
  423.4 1.0 constant_dynamic-update-slice_fusion.1
  425.4 1.0 fusion.59
  426.4 1.0 constant_dynamic-update-slice_fusion
  427.7 0.9 fusion.8
  428.6 0.8 copy.239
  429.3 1.9 fusion.93
  433.6 0.8 copy.252
  436.1 1.5 convolution_convert_fusion
  437.5 30.2 %reduce-scatter.2.cloned.1.call-done = bf16[512,256]{1,0:T(8,128)(2,1)} async-done(((bf16[512,1024]{1,0:T(8,128)(2,1)}), bf16[512,256]{1,0:T(8,128)(2,1)}) %reduce-scatter.2.cloned.1.call-update) | async-done | bytes 262160 | tf_op jit(solution)/shard_map/reduce_scatter | solution.py:203
  (139 shorter events, 17.9 us)
Async XLA Ops:
  6.5 461.3 %reduce-scatter.2.cloned.1.call-start = ((), (), s32[]{:S(2)}) async-start(), calls=%async_computation.1 | async-start | bytes 1310720 | tf_op jit(solution)/shard_map/reduce_scatter | solution.py:203
  119.4 1.0 copy-start.10
  223.2 1.8 copy-start
  223.2 1.8 copy-start.12
  225.0 1.1 copy-start.5
  225.3 1.5 copy-start.2
  231.1 17.7 %copy-start.16 = (f32[3,64]{1,0:T(4,128)S(1)}, f32[3,64]{1,0:T(4,128)}, u32[]{:S(2)}) copy-start(f32[3,64]{1,0:T(4,128)} %param.13) | copy-start | bytes 2308
  231.1 18.3 %copy-start.17 = (f32[3,64]{1,0:T(4,128)S(1)}, f32[3,64]{1,0:T(4,128)}, u32[]{:S(2)}) copy-start(f32[3,64]{1,0:T(4,128)} %param.14) | copy-start | bytes 2308
  231.1 18.8 %copy-start.13 = (bf16[2,64,8]{1,2,0:T(8,128)(2,1)S(1)}, bf16[2,64,8]{1,2,0:T(8,128)(2,1)}, u32[]{:S(2)}) copy-start(bf16[2,64,8]{1,2,0:T(8,128)(2,1)} %param.15) | copy-start | bytes 6148
  231.1 195.3 %collective-permute-start.5 = (bf16[4,128,2,128]{1,3,2,0:T(8,128)(2,1)}, bf16[4,128,2,128]{1,3,2,0:T(8,128)(2,1)}, u32[]{:S(2)}, u32[]{:S(2)}) collective-permute-start(bf16[4,128,2,128]{1,3,2,0:T(8,128)(2,1)} %get-tuple-element.13), channel_id=1, source_target_pairs={{8,0},{12,4},{16,8},{20,12},{24,16},{28,20},{32,24},{36,28},{40,32... | collective-permute-start | bytes 786440 | tf_op jit(solution)/shard_map/ppermute | solution.py:63
  235.1 178.4 %collective-permute-start.4 = (bf16[4,128,2,128]{1,3,2,0:T(8,128)(2,1)}, bf16[4,128,2,128]{1,3,2,0:T(8,128)(2,1)}, u32[]{:S(2)}, u32[]{:S(2)}) collective-permute-start(bf16[4,128,2,128]{1,3,2,0:T(8,128)(2,1)} %get-tuple-element.13), channel_id=1, source_target_pairs={{0,8},{4,12},{8,16},{12,20},{16,24},{20,28},{24,32},{28,36},{32,40... | collective-permute-start | bytes 786440 | tf_op jit(solution)/shard_map/ppermute | solution.py:63
  237.9 55.9 %copy-start.11 = (bf16[8,3,2,64]{3,2,1,0:T(2,128)(2,1)S(1)}, bf16[8,3,2,64]{3,2,1,0:T(2,128)(2,1)}, u32[]{:S(2)}) copy-start(bf16[8,3,2,64]{3,2,1,0:T(2,128)(2,1)} %param.10) | copy-start | bytes 18436
  237.9 170.5 %collective-permute-start = (bf16[4,32,2,128]{1,3,2,0:T(8,128)(2,1)S(1)}, bf16[4,32,2,128]{1,3,2,0:T(8,128)(2,1)}, u32[]{:S(2)}, u32[]{:S(2)}) collective-permute-start(bf16[4,32,2,128]{1,3,2,0:T(8,128)(2,1)S(1)} %get-tuple-element.20), channel_id=1, source_target_pairs={{0,4},{4,8},{8,12},{12,16},{16,20},{20,24},{24,28},{28,32},{32,36}... | collective-permute-start | bytes 196616 | tf_op jit(solution)/shard_map/ppermute | solution.py:51
  240.0 170.5 %collective-permute-start.1 = (bf16[4,32,2,128]{1,3,2,0:T(8,128)(2,1)}, bf16[4,32,2,128]{1,3,2,0:T(8,128)(2,1)}, u32[]{:S(2)}, u32[]{:S(2)}) collective-permute-start(bf16[4,32,2,128]{1,3,2,0:T(8,128)(2,1)} %get-tuple-element.21), channel_id=1, source_target_pairs={{4,0},{8,4},{12,8},{16,12},{20,16},{24,20},{28,24},{32,28},{36,32}... | collective-permute-start | bytes 196616 | tf_op jit(solution)/shard_map/ppermute | solution.py:53
  244.5 170.0 %collective-permute-start.3 = (bf16[4,128,2,2,128]{1,4,3,0,2:T(8,128)(2,1)}, bf16[4,128,2,2,128]{1,4,3,0,2:T(8,128)(2,1)}, u32[]{:S(2)}, u32[]{:S(2)}) collective-permute-start(bf16[4,128,2,2,128]{1,4,3,0,2:T(8,128)(2,1)} %fusion.43), channel_id=1, source_target_pairs={{4,0},{8,4},{12,8},{16,12},{20,16},{24,20},{28,24},{32,28},{36,32}... | collective-permute-start | bytes 1572872 | tf_op jit(solution)/shard_map/ppermute | solution.py:63
  397.2 1.8 copy-start.3
  400.8 0.8 copy-start.14
  401.6 0.7 copy-start.20
  401.7 1.3 copy-start.18
  401.7 1.9 copy-start.15
  405.5 6.4 %copy-start.6 = (f32[2,128,192]{1,2,0:T(8,128)S(1)}, f32[2,128,192]{1,2,0:T(8,128)}, u32[]{:S(2)}) copy-start(f32[2,128,192]{1,2,0:T(8,128)} %broadcast_multiply_fusion) | copy-start | bytes 589828
  405.5 6.4 %copy-start.8 = (pred[128,192]{0,1:T(8,128)(4,1)S(1)}, pred[128,192]{0,1:T(8,128)(4,1)}, u32[]{:S(2)}) copy-start(pred[128,192]{0,1:T(8,128)(4,1)} %fusion.71) | copy-start | bytes 73732
  405.5 6.4 %copy-start.19 = (f32[64]{0:T(128)S(1)}, f32[64]{0:T(128)}, u32[]{:S(2)}) copy-start(f32[64]{0:T(128)} %get-tuple-element.22) | copy-start | bytes 772
  408.4 11.5 %collective-permute-start.2 = (bf16[4,128,2,2,128]{1,4,3,0,2:T(8,128)(2,1)}, bf16[4,128,2,2,128]{1,4,3,0,2:T(8,128)(2,1)S(1)}, u32[]{:S(2)}, u32[]{:S(2)}) collective-permute-start(bf16[4,128,2,2,128]{1,4,3,0,2:T(8,128)(2,1)} %fusion.43), channel_id=1, source_target_pairs={{0,4},{4,8},{8,12},{12,16},{16,20},{20,24},{24,28},{28,32},{32,36}... | collective-permute-start | bytes 1572872 | tf_op jit(solution)/shard_map/ppermute | solution.py:63
  429.3 2.9 copy-start.7
  434.9 0.7 copy-start.9
  434.9 1.0 copy-start.1
  434.9 1.1 copy-start.4
Sparse Core Ops, SparseCore 0:
  437.7 30.0 reduce-scatter.1
where the time goes:
time: 475 us
  blocking collectives  356 us (75%)
  waiting for transfers between devices  34.6 us (7%)
  local copies, waits for them, and re-layouts  26.4 us (6%)
  starting transfers between devices  16.8 us (4%)
  other arithmetic  15.9 us (3%)
  between operations  14.2 us (3%)
  matrix products  10.5 us (2%)
    all_gather x9, blocking collectives, stacked_from(): tiles = lax.all_gather(tiles, axes[k], axis=0, tiled=True)  356 us
    reduce_scatter x1, waiting for transfers between devices, body(): lax.psum_scatter(terms.astype(jnp.bfloat16), 'tp', scatter_dimension=1, t...  30.2 us
    ppermute x4, starting transfers between devices, shifted(): return lax.ppermute(block, axis, route)  11.1 us
  transfers between devices with their start and end apart: 7, of which 2 were waited for; matrix products, arithmetic and copies ran while one was open for 6% of the time, Pallas kernels for 0%

commit v1 on v0

--- a/solution.py
+++ b/solution.py
@@ -24,7 +24,16 @@
 def stacked_from(value, axes, sequence):
     tiles = value[None]
     for k in sequence:
-        tiles = lax.all_gather(tiles, axes[k], axis=0, tiled=True)
+        take_the_sums_all = lambda frame, a_name: jnp.concatenate(
+            lax.all_to_all(
+                jnp.stack([frame for _ in range(lax.axis_size(a_name))]),
+                axis_name=a_name,
+                split_axis=0,
+                concat_axis=0,
+            ),
+            axis=0,
+        )
+        tiles = take_the_sums_all(tiles, axes[k])
     block = [lax.axis_size(axes[k]) for k in reversed(sequence)]
     tiles = tiles.reshape(*block, *value.shape)
     turned = sorted(range(len(sequence)), key=lambda place: sequence[len(sequence) - 1 - place])

time: 475 us -> 261 us (0.55)
  the two profiles are of different devices: /device:TPU:2 before, /device:TPU:4 now
where the time goes in v1:
time: 261 us; the launch traced here: 259 us
  waiting for transfers between devices  91.6 us (35%)
  starting transfers between devices  61.7 us (24%)
  local copies, waits for them, and re-layouts  43.3 us (17%)
  other arithmetic  21.2 us (8%)
  between operations  14.5 us (6%)
  blocking collectives  14.1 us (5%)
  matrix products  12.8 us (5%)
    all_to_all x6, waiting for transfers between devices, stacked_from(): lax.all_to_all(jnp.stack([frame for _ in range(lax.axis_size(a_name))]),...  50.4 us
    all_to_all x6, starting transfers between devices, stacked_from(): lax.all_to_all(jnp.stack([frame for _ in range(lax.axis_size(a_name))]),...  44.8 us
    reduce_scatter x1, waiting for transfers between devices, body(): lax.psum_scatter(terms.astype(jnp.bfloat16), 'tp', scatter_dimension=1, t...  37.9 us
    unnamed x83, local copies, waits for them, and re-layouts  17.7 us
    all_to_all x3, blocking collectives, stacked_from(): lax.all_to_all(jnp.stack([frame for _ in range(lax.axis_size(a_name))]),...  14.1 us
    ppermute x4, starting transfers between devices, shifted(): return lax.ppermute(block, axis, route)  11.2 us
    dot_general x3, matrix products, add_rows(): jnp.dot(columns, piece.reshape(rows, -1), preferred_element_type=jnp.floa...  5.51 us
    another operation x4, other arithmetic, stacked_from(): jnp.stack([frame for _ in range(lax.axis_size(a_name))])  5.26 us
  transfers between devices with their start and end apart: 13, of which 7 were waited for; matrix products, arithmetic and copies ran while one was open for 24% of the time, Pallas kernels for 0%

profile of v1, /device:TPU:4, one launch (start us, length us, event | category | flops | bytes accessed | tf_op | source)
XLA Modules:
  0.0 259.2 jit_solution(497345787227937397)
XLA Ops:
  7.9 15.2 %all-to-all-start.6 = ((bf16[16,1,128,8]{2,3,1,0:T(8,128)(2,1)}), bf16[16,1,128,8]{2,3,1,0:T(8,128)(2,1)S(1)}, u32[]{:S(2)}, u32[]{:S(2)}) async-start(bf16[16,1,128,8]{2,3,1,0:T(8,128)(2,1)} %stack.50), calls=%async_computation.6 | async-start | bytes 65536 | tf_op jit(solution)/shard_map/all_to_all | solution.py:28
  23.2 1.5 fusion.2
  24.7 1.1 stack.41
  25.9 1.2 reshape.599
  27.5 1.2 reshape.595
  28.8 6.9 %all-to-all-done.6 = bf16[16,1,128,8]{2,3,1,0:T(8,128)(2,1)S(1)} async-done(((bf16[16,1,128,8]{2,3,1,0:T(8,128)(2,1)}), bf16[16,1,128,8]{2,3,1,0:T(8,128)(2,1)S(1)}, u32[]{:S(2)}, u32[]{:S(2)}) %all-to-all-start.6) | async-done | bytes 32800 | tf_op jit(solution)/shard_map/all_to_all | solution.py:28
  36.4 4.8 %all-to-all-start.7 = ((bf16[4,16,128,8]{2,3,1,0:T(8,128)(2,1)}), bf16[4,16,128,8]{2,3,1,0:T(8,128)(2,1)S(1)}, u32[]{:S(2)}, u32[]{:S(2)}) async-start(bf16[4,16,128,8]{2,3,1,0:T(8,128)(2,1)} %stack.51), calls=%async_computation.7 | async-start | bytes 262144 | tf_op jit(solution)/shard_map/all_to_all | solution.py:28
  41.2 3.3 %all-to-all-done.7 = bf16[4,16,128,8]{2,3,1,0:T(8,128)(2,1)S(1)} async-done(((bf16[4,16,128,8]{2,3,1,0:T(8,128)(2,1)}), bf16[4,16,128,8]{2,3,1,0:T(8,128)(2,1)S(1)}, u32[]{:S(2)}, u32[]{:S(2)}) %all-to-all-start.7) | async-done | bytes 131104 | tf_op jit(solution)/shard_map/all_to_all | solution.py:28
  44.4 8.9 %all-to-all-start.2 = ((bf16[64,2,1536]{2,1,0:T(2,128)(2,1)}), bf16[64,2,1536]{2,1,0:T(2,128)(2,1)S(1)}, u32[]{:S(2)}, u32[]{:S(2)}) async-start(bf16[64,2,1536]{2,1,0:T(2,128)(2,1)} %reshape.599), calls=%async_computation.2 | async-start | bytes 786432 | tf_op jit(solution)/shard_map/all_to_all | solution.py:28
  54.6 23.8 %all-to-all-done.2 = bf16[64,2,1536]{2,1,0:T(2,128)(2,1)S(1)} async-done(((bf16[64,2,1536]{2,1,0:T(2,128)(2,1)}), bf16[64,2,1536]{2,1,0:T(2,128)(2,1)S(1)}, u32[]{:S(2)}, u32[]{:S(2)}) %all-to-all-start.2) | async-done | bytes 393248 | tf_op jit(solution)/shard_map/all_to_all | solution.py:28
  78.4 6.0 %all-to-all-start.4 = ((bf16[64,2,1536]{2,1,0:T(2,128)(2,1)}), bf16[64,2,1536]{2,1,0:T(2,128)(2,1)S(1)}, u32[]{:S(2)}, u32[]{:S(2)}) async-start(bf16[64,2,1536]{2,1,0:T(2,128)(2,1)} %reshape.595), calls=%async_computation.4 | async-start | bytes 786432 | tf_op jit(solution)/shard_map/all_to_all | solution.py:28
  84.8 1.2 reshape.603
  90.6 1.5 pad_maximum_fusion.1
  92.1 1.2 reshape.601
  93.4 16.3 %all-to-all-done.4 = bf16[64,2,1536]{2,1,0:T(2,128)(2,1)S(1)} async-done(((bf16[64,2,1536]{2,1,0:T(2,128)(2,1)}), bf16[64,2,1536]{2,1,0:T(2,128)(2,1)S(1)}, u32[]{:S(2)}, u32[]{:S(2)}) %all-to-all-start.4) | async-done | bytes 393248 | tf_op jit(solution)/shard_map/all_to_all | solution.py:28
  109.7 4.1 %all-to-all-start.8 = ((bf16[2,64,128,8]{2,3,1,0:T(8,128)(2,1)}), bf16[2,64,128,8]{2,3,1,0:T(8,128)(2,1)}, u32[]{:S(2)}, u32[]{:S(2)}) async-start(bf16[2,64,128,8]{2,3,1,0:T(8,128)(2,1)} %pad_maximum_fusion.6), calls=%async_computation.8 | async-start | bytes 524288 | tf_op jit(solution)/shard_map/all_to_all | solution.py:28
  114.3 1.5 pad_maximum_fusion.2
  115.8 2.0 reshape.597
  117.7 4.5 %all_to_all.45 = bf16[2,2,98304]{2,1,0:T(2,128)(2,1)S(1)} all-to-all(bf16[2,2,98304]{2,1,0:T(2,128)(2,1)S(1)} %reshape.601), channel_id=1, replica_groups=mesh['sp_0'=16,'sp_1'=4,'sp_2'=2,'tp'=4] {'sp_2'}, dimensions={0} | all-to-all | bytes 1572864 | tf_op jit(solution)/shard_map/all_to_all | solution.py:28
  122.3 5.3 %all_to_all.46 = bf16[2,2,98304]{2,1,0:T(2,128)(2,1)} all-to-all(bf16[2,2,98304]{2,1,0:T(2,128)(2,1)S(1)} %copy-done.1), channel_id=1, replica_groups=mesh['sp_0'=16,'sp_1'=4,'sp_2'=2,'tp'=4] {'sp_2'}, dimensions={0} | all-to-all | bytes 1572864 | tf_op jit(solution)/shard_map/all_to_all | solution.py:28
  127.5 6.0 %all-to-all-start = ((bf16[64,2,1536]{2,1,0:T(2,128)(2,1)}), bf16[64,2,1536]{2,1,0:T(2,128)(2,1)S(1)}, u32[]{:S(2)}, u32[]{:S(2)}) async-start(bf16[64,2,1536]{2,1,0:T(2,128)(2,1)} %reshape.603), calls=%async_computation | async-start | bytes 786432 | tf_op jit(solution)/shard_map/all_to_all | solution.py:28
  134.9 1.3 fusion.4
  136.1 1.7 copy.197
  138.9 1.1 copy.156
  140.0 1.7 reshape_reshape_reshape.10
  141.7 2.2 reshape.598
  143.9 1.1 copy.158
  145.0 1.7 reshape_reshape_reshape.11
  146.7 1.8 convolution_convert_fusion.2
  150.0 1.8 convolution_convert_fusion.1
  154.1 2.5 collective-permute-start.5
  156.6 3.4 %collective-permute-start.4 = (bf16[4,128,2,128]{1,3,2,0:T(8,128)(2,1)}, bf16[4,128,2,128]{1,3,2,0:T(8,128)(2,1)}, u32[]{:S(2)}, u32[]{:S(2)}) collective-permute-start(bf16[4,128,2,128]{1,3,2,0:T(8,128)(2,1)} %get-tuple-element.13), channel_id=1, source_target_pairs={{0,8},{4,12},{8,16},{12,20},{16,24},{20,28},{24,32},{28,36},{32,40... | collective-permute-start | bytes 786440 | tf_op jit(solution)/shard_map/ppermute | solution.py:72
  161.4 1.5 pad_maximum_fusion
  162.9 1.2 reshape.605
  164.1 4.4 %all_to_all.47 = bf16[2,2,98304]{2,1,0:T(2,128)(2,1)S(1)} all-to-all(bf16[2,2,98304]{2,1,0:T(2,128)(2,1)S(1)} %reshape.605), channel_id=1, replica_groups=mesh['sp_0'=16,'sp_1'=4,'sp_2'=2,'tp'=4] {'sp_2'}, dimensions={0} | all-to-all | bytes 1572864 | tf_op jit(solution)/shard_map/all_to_all | solution.py:28
  169.5 1.1 copy.154
  170.6 1.7 reshape_reshape_reshape.9
  172.3 1.8 convolution_convert_fusion.3
  175.7 2.1 collective-permute-start
  177.9 3.4 %collective-permute-start.1 = (bf16[4,32,2,128]{1,3,2,0:T(8,128)(2,1)S(1)}, bf16[4,32,2,128]{1,3,2,0:T(8,128)(2,1)S(1)}, u32[]{:S(2)}, u32[]{:S(2)}) collective-permute-start(bf16[4,32,2,128]{1,3,2,0:T(8,128)(2,1)S(1)} %get-tuple-element.21), channel_id=1, source_target_pairs={{4,0},{8,4},{12,8},{16,12},{20,16},{24,20},{28,24},{32,28},{36,32}... | collective-permute-start | bytes 196616 | tf_op jit(solution)/shard_map/ppermute | solution.py:62
  181.3 1.9 collective-permute-start.3
  183.3 1.0 multiply_multiply_fusion.1
  185.3 3.5 %collective-permute-start.2 = (bf16[4,128,2,2,128]{1,4,3,0,2:T(8,128)(2,1)S(1)}, bf16[4,128,2,2,128]{1,4,3,0,2:T(8,128)(2,1)S(1)}, u32[]{:S(2)}, u32[]{:S(2)}) collective-permute-start(bf16[4,128,2,2,128]{1,4,3,0,2:T(8,128)(2,1)S(1)} %copy-done.10), channel_id=1, source_target_pairs={{0,4},{4,8},{8,12},{12,16},{16,20},{20,24},{24,28},{28,32},{32,36}... | collective-permute-start | bytes 1572872 | tf_op jit(solution)/shard_map/ppermute | solution.py:72
  192.5 3.3 %collective-permute-done.2 = bf16[4,128,2,2,128]{1,4,3,0,2:T(8,128)(2,1)S(1)} collective-permute-done((bf16[4,128,2,2,128]{1,4,3,0,2:T(8,128)(2,1)S(1)}, bf16[4,128,2,2,128]{1,4,3,0,2:T(8,128)(2,1)S(1)}, u32[]{:S(2)}, u32[]{:S(2)}) %collective-permute-start.2) | collective-permute-done | bytes 524320 | tf_op jit(solution)/shard_map/ppermute | solution.py:72
  197.0 1.6 fusion.94
  204.1 1.9 fusion.93
  213.0 1.4 convolution_convert_fusion
  214.4 37.9 %reduce-scatter.2.cloned.1.call-done = bf16[512,256]{1,0:T(8,128)(2,1)} async-done(((bf16[512,1024]{1,0:T(8,128)(2,1)}), bf16[512,256]{1,0:T(8,128)(2,1)}) %reduce-scatter.2.cloned.1.call-update) | async-done | bytes 262160 | tf_op jit(solution)/shard_map/reduce_scatter | solution.py:212
  (187 shorter events, 37.1 us)
Async XLA Ops:
  7.9 27.8 %all-to-all-start.6 = ((bf16[16,1,128,8]{2,3,1,0:T(8,128)(2,1)}), bf16[16,1,128,8]{2,3,1,0:T(8,128)(2,1)S(1)}, u32[]{:S(2)}, u32[]{:S(2)}) async-start(bf16[16,1,128,8]{2,3,1,0:T(8,128)(2,1)} %stack.50), calls=%async_computation.6 | async-start | bytes 65536 | tf_op jit(solution)/shard_map/all_to_all | solution.py:28
  23.2 3.9 %copy-start.24 = (bf16[8,3,2,64]{3,2,1,0:T(2,128)(2,1)S(1)}, bf16[8,3,2,64]{3,2,1,0:T(2,128)(2,1)}, u32[]{:S(2)}) copy-start(bf16[8,3,2,64]{3,2,1,0:T(2,128)(2,1)} %param.12) | copy-start | bytes 18436
  27.5 25.8 %copy-start.30 = (f32[3,64]{1,0:T(4,128)S(1)}, f32[3,64]{1,0:T(4,128)}, u32[]{:S(2)}) copy-start(f32[3,64]{1,0:T(4,128)} %param.13) | copy-start | bytes 2308
  28.8 55.6 %copy-start.25 = (bf16[8,3,2,64]{3,2,1,0:T(2,128)(2,1)S(1)}, bf16[8,3,2,64]{3,2,1,0:T(2,128)(2,1)}, u32[]{:S(2)}) copy-start(bf16[8,3,2,64]{3,2,1,0:T(2,128)(2,1)} %param.10) | copy-start | bytes 18436
  36.4 8.1 %all-to-all-start.7 = ((bf16[4,16,128,8]{2,3,1,0:T(8,128)(2,1)}), bf16[4,16,128,8]{2,3,1,0:T(8,128)(2,1)S(1)}, u32[]{:S(2)}, u32[]{:S(2)}) async-start(bf16[4,16,128,8]{2,3,1,0:T(8,128)(2,1)} %stack.51), calls=%async_computation.7 | async-start | bytes 262144 | tf_op jit(solution)/shard_map/all_to_all | solution.py:28
  44.4 34.0 %all-to-all-start.2 = ((bf16[64,2,1536]{2,1,0:T(2,128)(2,1)}), bf16[64,2,1536]{2,1,0:T(2,128)(2,1)S(1)}, u32[]{:S(2)}, u32[]{:S(2)}) async-start(bf16[64,2,1536]{2,1,0:T(2,128)(2,1)} %reshape.599), calls=%async_computation.2 | async-start | bytes 786432 | tf_op jit(solution)/shard_map/all_to_all | solution.py:28
  78.4 31.2 %all-to-all-start.4 = ((bf16[64,2,1536]{2,1,0:T(2,128)(2,1)}), bf16[64,2,1536]{2,1,0:T(2,128)(2,1)S(1)}, u32[]{:S(2)}, u32[]{:S(2)}) async-start(bf16[64,2,1536]{2,1,0:T(2,128)(2,1)} %reshape.595), calls=%async_computation.4 | async-start | bytes 786432 | tf_op jit(solution)/shard_map/all_to_all | solution.py:28
  109.7 8.1 %all-to-all-start.8 = ((bf16[2,64,128,8]{2,3,1,0:T(8,128)(2,1)}), bf16[2,64,128,8]{2,3,1,0:T(8,128)(2,1)}, u32[]{:S(2)}, u32[]{:S(2)}) async-start(bf16[2,64,128,8]{2,3,1,0:T(8,128)(2,1)} %pad_maximum_fusion.6), calls=%async_computation.8 | async-start | bytes 524288 | tf_op jit(solution)/shard_map/all_to_all | solution.py:28
  117.7 4.5 %copy-start.1 = (bf16[2,2,98304]{2,1,0:T(2,128)(2,1)S(1)}, bf16[2,2,98304]{2,1,0:T(2,128)(2,1)}, u32[]{:S(2)}) copy-start(bf16[2,2,98304]{2,1,0:T(2,128)(2,1)} %reshape.597) | copy-start | bytes 2359300
  122.2 11.3 %copy-start.31 = (f32[3,64]{1,0:T(4,128)S(1)}, f32[3,64]{1,0:T(4,128)}, u32[]{:S(2)}) copy-start(f32[3,64]{1,0:T(4,128)} %param.14) | copy-start | bytes 2308
  122.2 11.9 %copy-start.15 = (f32[128,192]{0,1:T(8,128)S(1)}, f32[128,192]{0,1:T(8,128)}, u32[]{:S(2)}) copy-start(f32[128,192]{0,1:T(8,128)} %convert_multiply_fusion.10) | copy-start | bytes 294916
  122.2 12.6 %copy-start = (bf16[4,128,1024]{2,1,0:T(8,128)(2,1)S(1)}, bf16[4,128,1024]{2,1,0:T(8,128)(2,1)}, u32[]{:S(2)}) copy-start(bf16[4,128,1024]{2,1,0:T(8,128)(2,1)} %param.8) | copy-start | bytes 3145732
  122.2 12.6 %copy-start.26 = (f32[1024]{0:T(1024)S(1)}, f32[1024]{0:T(1024)}, u32[]{:S(2)}) copy-start(f32[1024]{0:T(1024)} %param.9) | copy-start | bytes 12292
  127.5 33.4 %all-to-all-start = ((bf16[64,2,1536]{2,1,0:T(2,128)(2,1)}), bf16[64,2,1536]{2,1,0:T(2,128)(2,1)S(1)}, u32[]{:S(2)}, u32[]{:S(2)}) async-start(bf16[64,2,1536]{2,1,0:T(2,128)(2,1)} %reshape.603), calls=%async_computation | async-start | bytes 786432 | tf_op jit(solution)/shard_map/all_to_all | solution.py:28
  133.5 118.8 %reduce-scatter.2.cloned.1.call-start = ((), (), s32[]{:S(2)}) async-start(), calls=%async_computation.10 | async-start | bytes 1310720 | tf_op jit(solution)/shard_map/reduce_scatter | solution.py:212
  145.0 1.7 copy-start.3
  148.5 1.4 copy-start.4
  154.1 47.7 %collective-permute-start.5 = (bf16[4,128,2,128]{1,3,2,0:T(8,128)(2,1)}, bf16[4,128,2,128]{1,3,2,0:T(8,128)(2,1)}, u32[]{:S(2)}, u32[]{:S(2)}) collective-permute-start(bf16[4,128,2,128]{1,3,2,0:T(8,128)(2,1)} %get-tuple-element.13), channel_id=1, source_target_pairs={{8,0},{12,4},{16,8},{20,12},{24,16},{28,20},{32,24},{36,28},{40,32... | collective-permute-start | bytes 786440 | tf_op jit(solution)/shard_map/ppermute | solution.py:72
  156.6 34.9 %collective-permute-start.4 = (bf16[4,128,2,128]{1,3,2,0:T(8,128)(2,1)}, bf16[4,128,2,128]{1,3,2,0:T(8,128)(2,1)}, u32[]{:S(2)}, u32[]{:S(2)}) collective-permute-start(bf16[4,128,2,128]{1,3,2,0:T(8,128)(2,1)} %get-tuple-element.13), channel_id=1, source_target_pairs={{0,8},{4,12},{8,16},{12,20},{16,24},{20,28},{24,32},{28,36},{32,40... | collective-permute-start | bytes 786440 | tf_op jit(solution)/shard_map/ppermute | solution.py:72
  170.6 1.7 copy-start.5
  174.2 0.8 copy-start.27
  175.1 6.2 %copy-start.10 = (bf16[4,128,2,2,128]{1,4,3,0,2:T(8,128)(2,1)S(1)}, bf16[4,128,2,2,128]{1,4,3,0,2:T(8,128)(2,1)}, u32[]{:S(2)}) copy-start(bf16[4,128,2,2,128]{1,4,3,0,2:T(8,128)(2,1)} %fusion.43) | copy-start | bytes 1572868
  175.4 9.0 %copy-start.28 = (f32[64]{0:T(128)S(1)}, f32[64]{0:T(128)}, u32[]{:S(2)}) copy-start(f32[64]{0:T(128)} %get-tuple-element.26) | copy-start | bytes 772
  175.7 9.5 %collective-permute-start = (bf16[4,32,2,128]{1,3,2,0:T(8,128)(2,1)S(1)}, bf16[4,32,2,128]{1,3,2,0:T(8,128)(2,1)S(1)}, u32[]{:S(2)}, u32[]{:S(2)}) collective-permute-start(bf16[4,32,2,128]{1,3,2,0:T(8,128)(2,1)S(1)} %get-tuple-element.20), channel_id=1, source_target_pairs={{0,4},{4,8},{8,12},{12,16},{16,20},{20,24},{24,28},{28,32},{32,36}... | collective-permute-start | bytes 196616 | tf_op jit(solution)/shard_map/ppermute | solution.py:60
  177.9 10.8 %collective-permute-start.1 = (bf16[4,32,2,128]{1,3,2,0:T(8,128)(2,1)S(1)}, bf16[4,32,2,128]{1,3,2,0:T(8,128)(2,1)S(1)}, u32[]{:S(2)}, u32[]{:S(2)}) collective-permute-start(bf16[4,32,2,128]{1,3,2,0:T(8,128)(2,1)S(1)} %get-tuple-element.21), channel_id=1, source_target_pairs={{4,0},{8,4},{12,8},{16,12},{20,16},{24,20},{28,24},{32,28},{36,32}... | collective-permute-start | bytes 196616 | tf_op jit(solution)/shard_map/ppermute | solution.py:62
  181.3 11.1 %collective-permute-start.3 = (bf16[4,128,2,2,128]{1,4,3,0,2:T(8,128)(2,1)S(1)}, bf16[4,128,2,2,128]{1,4,3,0,2:T(8,128)(2,1)S(1)}, u32[]{:S(2)}, u32[]{:S(2)}) collective-permute-start(bf16[4,128,2,2,128]{1,4,3,0,2:T(8,128)(2,1)S(1)} %copy-done.10), channel_id=1, source_target_pairs={{4,0},{8,4},{12,8},{16,12},{20,16},{24,20},{28,24},{32,28},{36,32}... | collective-permute-start | bytes 1572872 | tf_op jit(solution)/shard_map/ppermute | solution.py:72
  184.3 4.9 %copy-start.16 = (f32[2,128,192]{1,2,0:T(8,128)S(1)}, f32[2,128,192]{1,2,0:T(8,128)}, u32[]{:S(2)}) copy-start(f32[2,128,192]{1,2,0:T(8,128)} %broadcast_multiply_fusion) | copy-start | bytes 589828
  184.3 4.9 %copy-start.19 = (pred[128,192]{0,1:T(8,128)(4,1)S(1)}, pred[128,192]{0,1:T(8,128)(4,1)}, u32[]{:S(2)}) copy-start(pred[128,192]{0,1:T(8,128)(4,1)} %fusion.71) | copy-start | bytes 73732
  184.3 4.9 %copy-start.32 = (f32[64]{0:T(128)S(1)}, f32[64]{0:T(128)}, u32[]{:S(2)}) copy-start(f32[64]{0:T(128)} %get-tuple-element.22) | copy-start | bytes 772
  185.3 10.5 %collective-permute-start.2 = (bf16[4,128,2,2,128]{1,4,3,0,2:T(8,128)(2,1)S(1)}, bf16[4,128,2,2,128]{1,4,3,0,2:T(8,128)(2,1)S(1)}, u32[]{:S(2)}, u32[]{:S(2)}) collective-permute-start(bf16[4,128,2,2,128]{1,4,3,0,2:T(8,128)(2,1)S(1)} %copy-done.10), channel_id=1, source_target_pairs={{0,4},{4,8},{8,12},{12,16},{16,20},{20,24},{24,28},{28,32},{32,36}... | collective-permute-start | bytes 1572872 | tf_op jit(solution)/shard_map/ppermute | solution.py:72
  190.4 5.4 %copy-start.7 = (bf16[4,128,2,128]{1,3,2,0:T(8,128)(2,1)S(1)}, bf16[4,128,2,128]{1,3,2,0:T(8,128)(2,1)}, u32[]{:S(2)}) copy-start(bf16[4,128,2,128]{1,3,2,0:T(8,128)(2,1)} %get-tuple-element.14) | copy-start | bytes 786436
  192.4 3.5 %copy-start.11 = (bf16[4,128,2,2,128]{1,4,3,0,2:T(8,128)(2,1)}, bf16[4,128,2,2,128]{1,4,3,0,2:T(8,128)(2,1)S(1)}, u32[]{:S(2)}) copy-start(bf16[4,128,2,2,128]{1,4,3,0,2:T(8,128)(2,1)S(1)} %collective-permute-done.3) | copy-start | bytes 1572868
  195.7 0.8 copy-start.13
  196.0 0.9 copy-start.18
  196.0 0.9 copy-start.20
  196.9 2.8 %copy-start.14 = (bf16[4,128,2,2,128]{1,4,3,0,2:T(8,128)(2,1)S(1)}, bf16[4,128,2,2,128]{1,4,3,0,2:T(8,128)(2,1)}, u32[]{:S(2)}) copy-start(bf16[4,128,2,2,128]{1,4,3,0,2:T(8,128)(2,1)} %copy-done.13) | copy-start | bytes 1572868
  198.6 3.2 %copy-start.12 = (bf16[4,128,2,2,128]{1,4,3,0,2:T(8,128)(2,1)S(1)}, bf16[4,128,2,2,128]{1,4,3,0,2:T(8,128)(2,1)}, u32[]{:S(2)}) copy-start(bf16[4,128,2,2,128]{1,4,3,0,2:T(8,128)(2,1)} %copy-done.11) | copy-start | bytes 1572868
  199.8 3.3 %copy-start.29 = (f32[64]{0:T(128)S(1)}, f32[64]{0:T(128)}, u32[]{:S(2)}) copy-start(f32[64]{0:T(128)} %get-tuple-element.23) | copy-start | bytes 772
  206.0 3.6 %copy-start.8 = (f32[4,16,2,8,40]{4,3,2,1,0:T(8,128)}, f32[4,16,2,8,40]{4,3,2,1,0:T(8,128)S(1)}, u32[]{:S(2)}) copy-start(f32[4,16,2,8,40]{4,3,2,1,0:T(8,128)S(1)} %get-tuple-element.29) | copy-start | bytes 491524
  209.6 0.8 copy-start.17
  210.0 1.3 copy-start.9
  211.8 0.7 copy-start.21
  211.8 0.7 copy-start.22
  211.8 0.7 copy-start.23
  211.8 1.0 copy-start.2
  211.8 1.1 copy-start.6
Sparse Core Ops, SparseCore 0:
  214.5 37.7 reduce-scatter.1
